TPU v7x, 1024 devices: a whole 4x8x16 slice. The times are simulated.
1024 devices in a mesh: ep: 32 (over z, core), tp: 32 (over y, x).
Axes of the slice: x: 4, y: 8, z: 16, core: 2. Of those that a mesh axis runs over, the one named last changes fastest.
Arguments:
- tokens: bfloat16 [1536, 2048], P('ep', 'tp'), may hold values from -64 to 64
- mix_gain: float32 [2048], replicated, may hold values from 0.1 to 1.9
- w_gate_z: bfloat16 [2048, 2048], P(None, 'tp'), may hold values from -0.125 to 0.125
- w_value_x: bfloat16 [2048, 2048], P(None, 'tp'), may hold values from -0.125 to 0.125
- w_key_b: bfloat16 [2048, 256], replicated, may hold values from -0.125 to 0.125
- w_query_c: bfloat16 [2048, 256], replicated, may hold values from -0.125 to 0.125
- w_step: bfloat16 [2048, 32], replicated, may hold values from -0.125 to 0.125
- step_bias: float32 [32], replicated, may hold values from -2 to 1
- decay_log: float32 [32], replicated, may hold values from -3 to 1.4
- skip_gain: float32 [32], replicated, may hold values from 0.1 to 1.9
- conv_x_weight: bfloat16 [4, 2048], P(None, 'tp'), may hold values from -3 to 3
- conv_b_weight: bfloat16 [4, 256], replicated, may hold values from -3 to 3
- conv_c_weight: bfloat16 [4, 256], replicated, may hold values from -3 to 3
- window_x: bfloat16 [1536, 3, 2048], P('ep', None, 'tp'), may hold values from -6 to 6
- window_b: bfloat16 [1536, 3, 256], P('ep'), may hold values from -6 to 6
- window_c: bfloat16 [1536, 3, 256], P('ep'), may hold values from -6 to 6
- ssm_state: float32 [1536, 32, 64, 128], P('ep', 'tp'), may hold values from -2 to 2
- head_gain: float32 [2048], P('tp'), may hold values from 0.1 to 1.9
- w_out: bfloat16 [2048, 2048], P('tp'), may hold values from -0.25 to 0.25
- ffn_gain: float32 [2048], replicated, may hold values from 0.1 to 1.9
- route_ids: int32 [1536, 2], P('ep'), may hold values from 0 to 127, all different within a row; in each aligned block of 48 rows (0 to 47, 48 to 95, ...) at most 2 rows name the same one
- route_weights: float32 [1536, 2], P('ep'), may hold values from 0.05 to 1
- expert_gate: bfloat16 [32, 2048, 4096], P('ep', None, 'tp'), may hold values from -0.125 to 0.125
- expert_up: bfloat16 [32, 2048, 4096], P('ep', None, 'tp'), may hold values from -0.125 to 0.125
- expert_down: bfloat16 [32, 4096, 2048], P('ep', 'tp'), may hold values from -0.375 to 0.375
Outputs:
- layer_out: bfloat16 [1536, 2048], P('ep', 'tp')
Inputs may be any that keep to these rules, and one draw needn't show every extreme that they name: `route_ids`: each row names 2 different experts. Within the rows of one index of ep (aligned blocks of 48 rows) no expert is named by more than 2 rows, a bound that some block reaches.
All inputs are finite; a program needn't handle non-finite values.
Results may differ from a plain program's by a relative error of at most 0.009.
Values may be sent and summed in bfloat16 or wider, within the bound.
A program may use at most 32 MiB of HBM per device.

v0:
```python
import jax
import jax.numpy as jnp
from jax import lax
from jax.sharding import PartitionSpec as P

HEADS = 32
HEAD_DIM = 64
STATE = 128
GROUPS = 2
EXP_IN = 4


norm_epsilon = 1e-06


def sent_to_all(array, axis):
    copies = jnp.broadcast_to(array, (lax.axis_size(axis), *array.shape))
    return lax.all_to_all(copies, axis, split_axis=0, concat_axis=0, tiled=True)


def in_order(tiles, dim):
    dims = list(tiles.shape[1:])
    dims[dim] *= tiles.shape[0]
    return jnp.moveaxis(tiles, 0, dim).reshape(dims)


def gathered_copies(array, axis, dim):
    tiles = sent_to_all(array, axis)
    return in_order(tiles, dim)


def cut_along(array, dim, count):
    dims = array.shape
    tiles = array.reshape(*dims[:dim], count, dims[dim] // count, *dims[dim + 1 :])
    return jnp.moveaxis(tiles, dim, 0)


def sum_at_owner(array, axis, dim):
    count = lax.axis_size(axis)
    tiles = lax.all_to_all(cut_along(array, dim, count), axis, 0, 0, tiled=True)
    return jnp.sum(tiles, axis=0)


def summed_on_arrival(array, axis, dim):
    count = lax.axis_size(axis)
    tiles = lax.all_to_all(cut_along(array, dim, count), axis, 0, 0, tiled=True)
    return jnp.sum(tiles.astype(jnp.float32), axis=0)


def row_norm(arr_values, norm_gain):
    widened = arr_values.astype(jnp.float32)
    return (
        widened
        * lax.rsqrt(jnp.mean(widened * widened, axis=-1, keepdims=True) + norm_epsilon)
        * norm_gain
    )


def short_conv(window, fresh_row, weight):
    conv_taps = weight.astype(jnp.float32)
    summed = (
        jnp.sum(window.astype(jnp.float32) * conv_taps[:-1][None], axis=1)
        + fresh_row * conv_taps[-1]
    )
    return jax.nn.silu(summed)


def product(left, right):
    return jnp.dot(left, right, preferred_element_type=jnp.float32)


def local(
    tokens,
    mix_gain,
    w_gate_z,
    w_value_x,
    w_key_b,
    w_query_c,
    w_step,
    step_bias,
    decay_log,
    skip_gain,
    conv_x_weight,
    conv_b_weight,
    conv_c_weight,
    window_x,
    window_b,
    window_c,
    ssm_state,
    head_gain,
    w_out,
    ffn_gain,
    route_ids,
    route_weights,
    expert_gate,
    expert_up,
    expert_down,
):
    tp_index = lax.axis_index("tp")
    tp_count = lax.axis_size("tp")
    ep_count = lax.axis_size("ep")
    seq_count = tokens.shape[0]
    gathered = gathered_copies(tokens, "tp", 1)
    normed = row_norm(gathered, mix_gain).astype(jnp.bfloat16)
    local_width = w_gate_z.shape[1]
    head_count = local_width // HEAD_DIM
    first_head = tp_index * head_count
    group_start = first_head // (HEADS // GROUPS) * STATE
    gate_z = product(normed, w_gate_z)
    values = short_conv(window_x, product(normed, w_value_x), conv_x_weight)
    key_b = short_conv(
        lax.dynamic_slice_in_dim(window_b, group_start, STATE, 2),
        product(normed, lax.dynamic_slice_in_dim(w_key_b, group_start, STATE, 1)),
        lax.dynamic_slice_in_dim(conv_b_weight, group_start, STATE, 1),
    )
    query_c = short_conv(
        lax.dynamic_slice_in_dim(window_c, group_start, STATE, 2),
        product(normed, lax.dynamic_slice_in_dim(w_query_c, group_start, STATE, 1)),
        lax.dynamic_slice_in_dim(conv_c_weight, group_start, STATE, 1),
    )
    step_all = product(normed, w_step) + step_bias
    step_size = jax.nn.softplus(lax.dynamic_slice_in_dim(step_all, first_head, head_count, 1))
    rate_heads = jnp.exp(lax.dynamic_slice_in_dim(decay_log, first_head, head_count, 0))
    skip_heads = lax.dynamic_slice_in_dim(skip_gain, first_head, head_count, 0)
    decay_heads = jnp.exp(-step_size * rate_heads)
    value_heads = values.reshape(seq_count, head_count, HEAD_DIM)
    new_state = (
        decay_heads[:, :, None, None] * ssm_state
        + (step_size[:, :, None] * value_heads)[..., None] * key_b[:, None, None, :]
    )
    read_out = jnp.einsum("shpn,sn->shp", new_state, query_c, precision=lax.Precision.HIGHEST)
    read_out = read_out + skip_heads[None, :, None] * value_heads
    gated = read_out * jax.nn.silu(gate_z.reshape(seq_count, head_count, HEAD_DIM))
    gated = gated * lax.rsqrt(jnp.mean(gated * gated, axis=-1, keepdims=True) + norm_epsilon)
    mixed_heads = (
        (gated * head_gain.reshape(head_count, HEAD_DIM))
        .reshape(seq_count, local_width)
        .astype(jnp.bfloat16)
    )
    partial_value = product(mixed_heads, w_out)
    share_mix = sum_at_owner(partial_value, "tp", 1)
    residual_own = (tokens.astype(jnp.float32) + share_mix).astype(jnp.bfloat16)
    residual_full = gathered_copies(residual_own, "tp", 1)
    ffn_in = row_norm(residual_full, ffn_gain).astype(jnp.bfloat16)
    top_count = route_ids.shape[1]
    expert_count = EXP_IN * ep_count
    capacity = max(2, (3 * seq_count * top_count + 2 * expert_count - 1) // (2 * expert_count))
    sub_index = tp_index // (tp_count // EXP_IN)
    target_set = route_ids // EXP_IN
    hit_mask = route_ids % EXP_IN == sub_index
    set_grid = jnp.arange(ep_count, dtype=jnp.int32)
    set_onehot = (hit_mask[:, :, None] & (target_set[:, :, None] == set_grid)).astype(jnp.int32)
    set_onehot = set_onehot.reshape(seq_count * top_count, ep_count)
    earlier = jnp.cumsum(set_onehot, axis=0) - set_onehot
    slot_rank = jnp.sum(earlier * set_onehot, axis=1).reshape(seq_count, top_count)
    slot_index = jnp.where(hit_mask, target_set * capacity + slot_rank, -1)
    slot_grid = jnp.arange(ep_count * capacity, dtype=jnp.int32)
    slot_match = slot_index[:, :, None] == slot_grid
    placed = jnp.any(slot_match, axis=1).astype(jnp.bfloat16)
    outgoing = jnp.einsum("sj,sd->jd", placed, ffn_in, preferred_element_type=jnp.float32)
    outgoing = outgoing.astype(jnp.bfloat16).reshape(ep_count, capacity, ffn_in.shape[1])
    route_share = route_weights / jnp.sum(route_weights, axis=1, keepdims=True)
    combine_weight = jnp.sum(jnp.where(slot_match, route_share[:, :, None], 0.0), axis=1)
    arrived = lax.all_to_all(outgoing, "ep", split_axis=0, concat_axis=0, tiled=True)
    source_count, slot_count, row_width = arrived.shape
    flat_rows = arrived.reshape(source_count * slot_count, row_width)
    gate_part = product(flat_rows, expert_gate[0])
    up_part = product(flat_rows, expert_up[0])
    hidden = (jax.nn.silu(gate_part) * up_part).astype(jnp.bfloat16)
    expert_out = product(hidden, expert_down[0]).reshape(source_count, slot_count, row_width)
    returned = lax.all_to_all(
        expert_out.astype(jnp.bfloat16), "ep", split_axis=0, concat_axis=0, tiled=True
    ).astype(expert_out.dtype)
    moe_part = jnp.dot(
        combine_weight,
        returned.reshape(ep_count * capacity, -1),
        precision=lax.Precision.HIGHEST,
        preferred_element_type=jnp.float32,
    )
    moe_share = summed_on_arrival(moe_part.astype(jnp.bfloat16), "tp", 1)
    return (residual_own.astype(jnp.float32) + moe_share).astype(jnp.bfloat16)


def solution(mesh):
    in_specs = (
        P("ep", "tp"),
        P(),
        P(None, "tp"),
        P(None, "tp"),
        P(),
        P(),
        P(),
        P(),
        P(),
        P(),
        P(None, "tp"),
        P(),
        P(),
        P("ep", None, "tp"),
        P("ep", None, None),
        P("ep", None, None),
        P("ep", "tp", None, None),
        P("tp"),
        P("tp", None),
        P(),
        P("ep", None),
        P("ep", None),
        P("ep", None, "tp"),
        P("ep", None, "tp"),
        P("ep", "tp", None),
    )
    out_specs = P("ep", "tp")
    return jax.shard_map(local, mesh=mesh, in_specs=in_specs, out_specs=out_specs, check_vma=False)
```

profile of v0, /device:TPU:1, one launch (start us, length us, event | category | flops | bytes accessed | tf_op | source)
XLA Modules:
  0.0 160.2 jit_solution(12800150877031927913)
XLA Ops:
  0.0 0.9 broadcast_in_dim.13
  0.9 0.9 reshape.130
  1.8 10.5 %all-to-all-start = ((bf16[32,2,1536]{2,1,0:T(2,128)(2,1)}), bf16[32,2,1536]{2,1,0:T(2,128)(2,1)S(1)}, u32[]{:S(2)}, u32[]{:S(2)}) async-start(bf16[32,2,1536]{2,1,0:T(2,128)(2,1)} %reshape.130), calls=%async_computation | async-start | bytes 393216 | tf_op jit(solution)/shard_map/all_to_all | solution.py:18
  12.3 0.7 fusion.39
  13.0 0.7 fusion.40
  13.7 0.7 slice.18
  14.4 0.8 multiply_reduce_fusion.2
  15.2 0.7 convert_element_type.95
  15.9 1.3 dynamic_slice.35
  17.2 1.2 dynamic_slice.28
  19.1 1.3 dynamic-slice
  20.4 0.3 copy.77
  20.7 1.5 all-to-all-done
  22.2 0.3 reshape.131
  22.8 0.3 copy.61
  23.1 0.3 reshape.124
  23.9 0.2 divide_multiply_fusion
  24.1 1.3 divide_multiply_fusion.1
  25.5 0.7 exponential_bitcast_fusion
  26.2 0.2 broadcast_multiply_fusion
  26.4 2.7 %fusion = f32[48,1,64]{2,1,0:T(1,128)S(1)} fusion(f32[48,128,1]{1,2,0:T(1,128)S(1)} %bitcast.64, f32[48,1,64,128]{3,2,1,0:T(8,128)S(1)} %copy-done.1, f32[48,128]{1,0:T(8,128)S(1)} %divide_multiply_fusion.1, f32[48,64]{1,0:T(8,128)S(1)} %get-tuple-element.9, f32[48]{0:T(128)S(1)} %get-tuple-element.7), kind=kOutput, calls=%fused_computation.3 | convolution fusion | flops 5898240 | bytes 1646784 | tf_op jit(solution)/shard_map/shpn,sn->shp/dot_general | solution.py:131
  29.1 1.0 multiply_reduce_fusion.3
  30.1 0.6 convolution_bitcast_fusion
  30.7 1.2 reshape.132
  31.9 7.8 %all-to-all-start.1 = ((f32[32,1,3072]{2,1,0:T(1,128)}), f32[32,1,3072]{2,1,0:T(1,128)S(1)}, u32[]{:S(2)}, u32[]{:S(2)}) async-start(f32[32,1,3072]{2,1,0:T(1,128)} %reshape.132), calls=%async_computation.1 | async-start | bytes 786432 | tf_op jit(solution)/shard_map/all_to_all | solution.py:40
  40.5 10.7 %all-to-all-done.1 = f32[32,1,3072]{2,1,0:T(1,128)S(1)} async-done(((f32[32,1,3072]{2,1,0:T(1,128)}), f32[32,1,3072]{2,1,0:T(1,128)S(1)}, u32[]{:S(2)}, u32[]{:S(2)}) %all-to-all-start.1) | async-done | bytes 393248 | tf_op jit(solution)/shard_map/all_to_all | solution.py:40
  51.2 0.5 broadcast.121
  51.7 1.6 reduce.6
  53.6 0.9 reshape.134
  54.5 3.9 %all-to-all-start.2 = ((bf16[32,2,1536]{2,1,0:T(2,128)(2,1)}), bf16[32,2,1536]{2,1,0:T(2,128)(2,1)S(1)}, u32[]{:S(2)}, u32[]{:S(2)}) async-start(bf16[32,2,1536]{2,1,0:T(2,128)(2,1)} %reshape.134), calls=%async_computation.2 | async-start | bytes 393216 | tf_op jit(solution)/shard_map/all_to_all | solution.py:18
  59.0 9.4 %all-to-all-done.2 = bf16[32,2,1536]{2,1,0:T(2,128)(2,1)S(1)} async-done(((bf16[32,2,1536]{2,1,0:T(2,128)(2,1)}), bf16[32,2,1536]{2,1,0:T(2,128)(2,1)S(1)}, u32[]{:S(2)}, u32[]{:S(2)}) %all-to-all-start.2) | async-done | bytes 196640 | tf_op jit(solution)/shard_map/all_to_all | solution.py:18
  68.3 0.3 reshape.135
  68.9 0.3 copy.71
  69.2 0.3 reshape.125
  69.6 0.3 convolution_convert_fusion.1
  70.1 47.4 %all_to_all.30 = bf16[32,2,2048]{2,1,0:T(2,128)(2,1)S(1)} all-to-all(bf16[32,2,2048]{2,1,0:T(2,128)(2,1)S(1)} %reshape.120), channel_id=1, replica_groups=mesh['ep'=32,'tp'=32] {'ep'}, dimensions={0} | all-to-all | bytes 524288 | tf_op jit(solution)/shard_map/all_to_all | solution.py:164
  117.6 0.2 fusion.16
  117.9 0.2 fusion.5
  118.1 0.2 convolution_convert_fusion
  118.3 1.0 copy.73
  119.3 4.2 %all-to-all-start.4 = ((bf16[32,2,2048]{2,1,0:T(2,128)(2,1)}), bf16[32,2,2048]{2,1,0:T(2,128)(2,1)S(1)}, u32[]{:S(2)}, u32[]{:S(2)}) async-start(bf16[32,2,2048]{2,1,0:T(2,128)(2,1)} %copy.73), calls=%async_computation.4 | async-start | bytes 524288 | tf_op jit(solution)/shard_map/all_to_all | solution.py:171
  123.6 21.5 %all-to-all-done.4 = bf16[32,2,2048]{2,1,0:T(2,128)(2,1)S(1)} async-done(((bf16[32,2,2048]{2,1,0:T(2,128)(2,1)}), bf16[32,2,2048]{2,1,0:T(2,128)(2,1)S(1)}, u32[]{:S(2)}, u32[]{:S(2)}) %all-to-all-start.4) | async-done | bytes 262176 | tf_op jit(solution)/shard_map/all_to_all | solution.py:171
  145.2 0.3 convolution_convert_fusion.2
  145.5 0.4 reshape.123
  146.1 0.2 reshape.136
  146.3 12.9 %all_to_all.31 = bf16[32,2,1536]{2,1,0:T(2,128)(2,1)S(1)} all-to-all(bf16[32,2,1536]{2,1,0:T(2,128)(2,1)S(1)} %reshape.136), channel_id=1, replica_groups=mesh['ep'=32,'tp'=32] {'tp'}, dimensions={0} | all-to-all | bytes 393216 | tf_op jit(solution)/shard_map/all_to_all | solution.py:46
  159.2 0.3 reshape.137
  159.6 0.6 add_convert_fusion
  (73 shorter events, 3.6 us)
Async XLA Ops:
  0.0 23.9 %copy-start = (bf16[2048,256]{1,0:T(8,128)(2,1)S(1)}, bf16[2048,256]{1,0:T(8,128)(2,1)}, u32[]{:S(2)}) copy-start(bf16[2048,256]{1,0:T(8,128)(2,1)} %param.30) | copy-start | bytes 3145732
  0.0 20.4 %copy-start.5 = (bf16[64,2048]{1,0:T(8,128)(2,1)S(1)}, bf16[64,2048]{1,0:T(8,128)(2,1)}, u32[]{:S(2)}) copy-start(bf16[64,2048]{1,0:T(8,128)(2,1)} %param.43) | copy-start | bytes 786436
  0.0 20.6 %copy-start.10 = (bf16[48,3,256]{2,0,1:T(8,128)(2,1)S(1)}, bf16[48,3,256]{2,0,1:T(8,128)(2,1)}, u32[]{:S(2)}) copy-start(bf16[48,3,256]{2,0,1:T(8,128)(2,1)} %param.40) | copy-start | bytes 221188
  0.0 20.6 %copy-start.11 = (bf16[48,3,256]{2,0,1:T(8,128)(2,1)S(1)}, bf16[48,3,256]{2,0,1:T(8,128)(2,1)}, u32[]{:S(2)}) copy-start(bf16[48,3,256]{2,0,1:T(8,128)(2,1)} %param.39) | copy-start | bytes 221188
  1.8 20.4 %all-to-all-start = ((bf16[32,2,1536]{2,1,0:T(2,128)(2,1)}), bf16[32,2,1536]{2,1,0:T(2,128)(2,1)S(1)}, u32[]{:S(2)}, u32[]{:S(2)}) async-start(bf16[32,2,1536]{2,1,0:T(2,128)(2,1)} %reshape.130), calls=%async_computation | async-start | bytes 393216 | tf_op jit(solution)/shard_map/all_to_all | solution.py:18
  22.7 0.7 copy-start.12
  22.8 0.9 copy-start.8
  23.0 3.1 %copy-start.6 = (bf16[2048,64]{0,1:T(8,128)(2,1)S(1)}, bf16[2048,64]{0,1:T(8,128)(2,1)}, u32[]{:S(2)}) copy-start(bf16[2048,64]{0,1:T(8,128)(2,1)} %param.28) | copy-start | bytes 786436
  23.4 3.0 %copy-start.1 = (f32[48,1,64,128]{3,2,1,0:T(8,128)S(1)}, f32[48,1,64,128]{3,2,1,0:T(8,128)}, u32[]{:S(2)}) copy-start(f32[48,1,64,128]{3,2,1,0:T(8,128)} %param.41) | copy-start | bytes 4718596
  24.1 5.0 %copy-start.7 = (bf16[2048,64]{0,1:T(8,128)(2,1)S(1)}, bf16[2048,64]{0,1:T(8,128)(2,1)}, u32[]{:S(2)}) copy-start(bf16[2048,64]{0,1:T(8,128)(2,1)} %param.27) | copy-start | bytes 786436
  25.5 4.6 %copy-start.16 = (f32[64]{0:T(128)S(1)}, f32[64]{0:T(128)}, u32[]{:S(2)}) copy-start(f32[64]{0:T(128)} %param.42) | copy-start | bytes 772
  30.1 9.6 %copy-start.15 = (s32[48,2]{0,1:T(2,128)S(1)}, s32[48,2]{0,1:T(2,128)}, u32[]{:S(2)}) copy-start(s32[48,2]{0,1:T(2,128)} %param.45) | copy-start | bytes 1156
  31.9 19.2 %all-to-all-start.1 = ((f32[32,1,3072]{2,1,0:T(1,128)}), f32[32,1,3072]{2,1,0:T(1,128)S(1)}, u32[]{:S(2)}, u32[]{:S(2)}) async-start(f32[32,1,3072]{2,1,0:T(1,128)} %reshape.132), calls=%async_computation.1 | async-start | bytes 786432 | tf_op jit(solution)/shard_map/all_to_all | solution.py:40
  39.7 13.8 %copy-start.9 = (bf16[48,64]{1,0:T(8,128)(2,1)S(1)}, bf16[48,64]{1,0:T(8,128)(2,1)}, u32[]{:S(2)}) copy-start(bf16[48,64]{1,0:T(8,128)(2,1)} %param.25) | copy-start | bytes 18436
  54.5 13.8 %all-to-all-start.2 = ((bf16[32,2,1536]{2,1,0:T(2,128)(2,1)}), bf16[32,2,1536]{2,1,0:T(2,128)(2,1)S(1)}, u32[]{:S(2)}, u32[]{:S(2)}) async-start(bf16[32,2,1536]{2,1,0:T(2,128)(2,1)} %reshape.134), calls=%async_computation.2 | async-start | bytes 393216 | tf_op jit(solution)/shard_map/all_to_all | solution.py:18
  68.9 0.7 copy-start.13
  69.2 48.5 %copy-start.2 = (bf16[1,2048,128]{2,1,0:T(8,128)(2,1)S(1)}, bf16[1,2048,128]{2,1,0:T(8,128)(2,1)}, u32[]{:S(2)}) copy-start(bf16[1,2048,128]{2,1,0:T(8,128)(2,1)} %param.47) | copy-start | bytes 1572868
  69.6 48.3 %copy-start.3 = (bf16[1,2048,128]{2,1,0:T(8,128)(2,1)S(1)}, bf16[1,2048,128]{2,1,0:T(8,128)(2,1)}, u32[]{:S(2)}) copy-start(bf16[1,2048,128]{2,1,0:T(8,128)(2,1)} %param.48) | copy-start | bytes 1572868
  69.9 48.2 %copy-start.4 = (bf16[1,128,2048]{2,1,0:T(8,128)(2,1)S(1)}, bf16[1,128,2048]{2,1,0:T(8,128)(2,1)}, u32[]{:S(2)}) copy-start(bf16[1,128,2048]{2,1,0:T(8,128)(2,1)} %param.49) | copy-start | bytes 1572868
  117.6 5.9 %copy-start.14 = (f32[48,2]{0,1:T(2,128)S(1)}, f32[48,2]{0,1:T(2,128)}, u32[]{:S(2)}) copy-start(f32[48,2]{0,1:T(2,128)} %param.46) | copy-start | bytes 1156
  119.3 25.8 %all-to-all-start.4 = ((bf16[32,2,2048]{2,1,0:T(2,128)(2,1)}), bf16[32,2,2048]{2,1,0:T(2,128)(2,1)S(1)}, u32[]{:S(2)}, u32[]{:S(2)}) async-start(bf16[32,2,2048]{2,1,0:T(2,128)(2,1)} %copy.73), calls=%async_computation.4 | async-start | bytes 524288 | tf_op jit(solution)/shard_map/all_to_all | solution.py:171
where the time goes:
time: 162 us; the launch traced here: 160 us
  blocking collectives  60.3 us (37%)
  waiting for transfers between devices  43 us (27%)
  starting transfers between devices  26.3 us (16%)
  local copies, waits for them, and re-layouts  14.6 us (9%)
  matrix products  7.49 us (5%)
  other arithmetic  7.21 us (4%)
    all_to_all x1, blocking collectives, local(): lax.all_to_all(outgoing, 'ep', split_axis=0, concat_axis=0, tiled=True)  47.4 us
    all_to_all x1, waiting for transfers between devices, local(): lax.all_to_all(expert_out.astype(jnp.bfloat16), 'ep', split_axis=0, conca...  21.5 us
    all_to_all x2, starting transfers between devices, sent_to_all(): return lax.all_to_all(copies, axis, split_axis=0, concat_axis=0, tiled=True)  14.4 us
    all_to_all x1, blocking collectives, summed_on_arrival(): tiles = lax.all_to_all(cut_along(array, dim, count), axis, 0, 0, tiled=True)  12.9 us
    all_to_all x2, waiting for transfers between devices, sent_to_all(): return lax.all_to_all(copies, axis, split_axis=0, concat_axis=0, tiled=True)  10.8 us
    all_to_all x1, waiting for transfers between devices, sum_at_owner(): tiles = lax.all_to_all(cut_along(array, dim, count), axis, 0, 0, tiled=True)  10.7 us
    all_to_all x1, starting transfers between devices, sum_at_owner(): tiles = lax.all_to_all(cut_along(array, dim, count), axis, 0, 0, tiled=True)  7.75 us
    unnamed x43, local copies, waits for them, and re-layouts  4.87 us
  transfers between devices with their start and end apart: 4, of which 4 were waited for; matrix products, arithmetic and copies ran while one was open for 6% of the time, Pallas kernels for 0%

commit v1 on v0

v1 whole, which is shorter than its diff:
```python
import functools

import jax
import jax.numpy as jnp
from jax import lax
from jax.experimental import pallas as pl
from jax.experimental.pallas import tpu as pltpu
from jax.sharding import PartitionSpec as P

MESH = pl.DeviceIdType.MESH
NX = 4
HEAD_DIM = 64
STATE = 128
GROUPS = 2
EXP_IN = 4
EPS = 1e-06
F32 = jnp.float32
BF16 = jnp.bfloat16


def far_first(i, n):
    half = (i + 1) // 2
    return n // 2 + half * (1 - 2 * (i % 2))


def silu(v):
    return v / (1.0 + jnp.exp(-v))


def dot(a, b):
    return lax.dot_general(a, b, (((1,), (0,)), ((), ())), preferred_element_type=F32)


def dot_nt(a, b):
    return lax.dot_general(a, b, (((1,), (1,)), ((), ())), preferred_element_type=F32)


def kernel(ne, nt, nx, rows, *refs):
    (
        tokens, mix_gain, w_gate, w_value, w_key, w_query, w_step, step_bias, decay_log, skip_gain,
        conv_x, conv_b, conv_c, window_x, window_b, window_c, state, head_gain, w_out, ffn_gain,
        route_ids, route_weights, e_gate, e_up, e_down,
        out_ref,
        tok_v, mg_v, wgv_v, wkq_v, bias_v, dlog_v, skip_v, cx_v, cb_v, cc_v, wx_v, wb_v, wc_v,
        st_v, hg_v, wo_v, fg_v, ids_v, rw_v, eg_v, eu_v, ed_v,
        s1, g1, s2, r2, s3f, s3, r3, r3f, s4, g4, s5, r5, s6f, s6, r6,
        nbuf, part, sh_v, sl_v, pt_v, pk_v,
        load_sem, send_sem, recv_sem,
    ) = refs
    ep = lax.axis_index("ep")
    tp = lax.axis_index("tp")
    ny = nt // nx
    half = rows // 2
    width = nt * HEAD_DIM
    experts = EXP_IN * ne
    share_tp = nt // EXP_IN
    group = tp // (nt // GROUPS)
    gcol = pl.multiple_of(group * STATE, STATE)

    def tp_peer(i):
        y = (tp // nx + far_first(i // nx, ny)) % ny
        x = (tp % nx + far_first(i % nx, nx)) % nx
        return y * nx + x

    def ep_peer(i):
        z = (ep // 2 + far_first(i // 2, ne // 2)) % (ne // 2)
        return z * 2 + (ep % 2 + 1 - i % 2) % 2

    loads = []

    def load(src, dst):
        copy = pltpu.make_async_copy(src, dst, load_sem.at[len(loads)])
        copy.start()
        loads.append(copy)
        return copy

    load_tok = load(tokens, tok_v)
    barrier = pltpu.get_barrier_semaphore()

    def greet_tp(i, c):
        pl.semaphore_signal(barrier, inc=1, device_id={"tp": tp_peer(i)}, device_id_type=MESH)
        return c

    def greet_ep(i, c):
        pl.semaphore_signal(barrier, inc=1, device_id={"ep": ep_peer(i)}, device_id_type=MESH)
        return c

    lax.fori_loop(0, ne - 1, greet_ep, 0)
    lax.fori_loop(0, nt - 1, greet_tp, 0)

    load_ids = load(route_ids, ids_v)
    load_rw = load(route_weights, rw_v)
    load_state = load(state, st_v)
    load_win = [
        load(window_x, wx_v),
        load(window_b.at[:, :, pl.ds(gcol, STATE)], wb_v),
        load(window_c.at[:, :, pl.ds(gcol, STATE)], wc_v),
        load(conv_x, cx_v),
        load(conv_b.at[:, pl.ds(gcol, STATE)], cb_v),
        load(conv_c.at[:, pl.ds(gcol, STATE)], cc_v),
    ]
    load_mix = [
        load(mix_gain, mg_v),
        load(w_gate, wgv_v.at[pl.ds(0, HEAD_DIM)]),
        load(w_value, wgv_v.at[pl.ds(HEAD_DIM, HEAD_DIM)]),
        load(w_step, wgv_v.at[pl.ds(2 * HEAD_DIM, w_step.shape[0])]),
        load(w_key.at[:, pl.ds(gcol, STATE)], wkq_v.at[:, pl.ds(0, STATE)]),
        load(w_query.at[:, pl.ds(gcol, STATE)], wkq_v.at[:, pl.ds(STATE, STATE)]),
        load(step_bias, bias_v),
        load(decay_log, dlog_v),
        load(skip_gain, skip_v),
        load(head_gain, hg_v),
        load(w_out, wo_v),
    ]
    load_ffn = [load(ffn_gain, fg_v), load(e_gate, eg_v), load(e_up, eu_v), load(e_down, ed_v)]

    low = lax.broadcasted_iota(jnp.int32, (1, 2 * HEAD_DIM), 1) < HEAD_DIM

    def swap(a):
        return pltpu.roll(a, HEAD_DIM, 1)

    def unpack(a, b):
        top = jnp.where(low, a, swap(b))
        bottom = jnp.where(low, swap(a), b)
        return jnp.concatenate([top, bottom], axis=0)

    def pack(block):
        n = block.shape[0] // 2
        top, bottom = block[:n], block[n:]
        return jnp.where(low, top, swap(bottom)), jnp.where(low, swap(top), bottom)

    def exchange(phase, axis, peer_of, count, source, target, me):
        def send(i, c):
            peer = peer_of(i)
            pltpu.make_async_remote_copy(
                src_ref=source(peer),
                dst_ref=target.at[me],
                send_sem=send_sem.at[phase],
                recv_sem=recv_sem.at[phase],
                device_id={axis: peer},
                device_id_type=MESH,
            ).start()
            return c

        lax.fori_loop(0, count - 1, send, 0)

    def landed(phase, target, count, sem):
        some = target.at[pl.ds(0, count - 1)]
        pltpu.make_async_copy(some, some, sem.at[phase]).wait()

    load_tok.wait()
    tok = tok_v[...].astype(F32)
    tok_packed = jnp.concatenate([tok[:half], tok[half:]], axis=1)
    s1[...] = tok_packed.astype(BF16)
    g1[tp] = tok_packed.astype(BF16)
    pl.semaphore_wait(barrier, ne - 1 + nt - 1)
    exchange(0, "tp", tp_peer, nt, lambda peer: s1, g1, tp)

    load_ids.wait()
    load_rw.wait()
    line = lax.broadcasted_iota(jnp.int32, (experts, rows), 0)
    expert_of = (line % ne) * EXP_IN + line // ne
    ids = ids_v[...]
    hit = [(ids[k : k + 1] == expert_of).astype(F32) for k in range(2)]
    named = (hit[0] + hit[1]).astype(BF16)
    before = (
        lax.broadcasted_iota(jnp.int32, (rows, rows), 0) < lax.broadcasted_iota(jnp.int32, (rows, rows), 1)
    ).astype(BF16)
    earlier = dot(named, before)
    rank = [(earlier < 0.5).astype(F32), (earlier > 0.5).astype(F32)]
    for r in range(2):
        pt_v[:, r * rows : (r + 1) * rows] = (named.astype(F32) * rank[r]).astype(BF16)
    for k in range(2):
        for r in range(2):
            pk_v[k * rows : (k + 1) * rows, r * experts : (r + 1) * experts] = (
                jnp.transpose(hit[k] * rank[r]).astype(BF16)
            )
    rw = rw_v[...]
    share = rw / jnp.sum(rw, axis=0, keepdims=True)
    eye = (
        lax.broadcasted_iota(jnp.int32, (rows, rows), 0) == lax.broadcasted_iota(jnp.int32, (rows, rows), 1)
    )
    share_col = [
        jnp.sum(jnp.where(eye, share[k : k + 1], 0.0), axis=1, keepdims=True) for k in range(2)
    ]
    load_state.wait()
    st = st_v[...]
    st_high = st.astype(BF16)
    sh_v[...] = st_high
    sl_v[...] = (st - st_high.astype(F32)).astype(BF16)
    for copy in load_win:
        copy.wait()

    def taps(window, weight):
        w = weight[...].astype(F32)
        total = window[0].astype(F32) * w[0:1]
        for j in range(1, 3):
            total = total + window[j].astype(F32) * w[j : j + 1]
        return total, w[3:4]

    past_x, tap_x = taps(wx_v, cx_v)
    past_b, tap_b = taps(wb_v, cb_v)
    past_c, tap_c = taps(wc_v, cc_v)
    for copy in load_mix:
        copy.wait()
    mine = lax.broadcasted_iota(jnp.int32, (1, nt), 1) == tp

    def head_scalar(ref):
        return jnp.sum(jnp.where(mine, ref[...], 0.0), axis=1, keepdims=True)

    bias = head_scalar(bias_v)
    decay_rate = jnp.exp(head_scalar(dlog_v))
    skip = head_scalar(skip_v)

    landed(0, g1, nt, recv_sem)
    blocks = []
    square = jnp.zeros((rows, 2 * HEAD_DIM), F32)
    for i in range(nt // 2):
        block = unpack(g1[2 * i].astype(F32), g1[2 * i + 1].astype(F32))
        square = square + block * block
        blocks.append(block)
    scale = lax.rsqrt(jnp.sum(square, axis=1, keepdims=True) / width + EPS)
    for i, block in enumerate(blocks):
        cols = slice(128 * i, 128 * i + 128)
        nbuf[:, cols] = (block * scale * mg_v[:, cols]).astype(BF16)
    normed = nbuf[...]
    kq = dot(normed, wkq_v[...])
    gvs = dot_nt(normed, wgv_v[...])
    gate_z = gvs[:, :HEAD_DIM]
    raw_v = gvs[:, HEAD_DIM : 2 * HEAD_DIM]
    keys = silu(past_b + kq[:, :STATE] * tap_b)
    queries = silu(past_c + kq[:, STATE:] * tap_c)
    values = silu(past_x + raw_v * tap_x)
    step_in = jnp.sum(jnp.where(mine, gvs[:, 2 * HEAD_DIM :], 0.0), axis=1, keepdims=True) + bias
    step = jnp.maximum(step_in, 0.0) + jnp.log1p(jnp.exp(-jnp.abs(step_in)))
    decay = jnp.exp(-step * decay_rate)
    key_query = jnp.sum(keys * queries, axis=1, keepdims=True)
    q_high = queries.astype(BF16)
    q_low = (queries - q_high.astype(F32)).astype(BF16)
    pieces = []
    unit = min(8, rows)
    for g in range(rows // unit):
        seqs = slice(g * unit, (g + 1) * unit)
        lines = slice(g * unit * HEAD_DIM, (g + 1) * unit * HEAD_DIM)
        high = sh_v[lines]
        prod = dot_nt(q_high[seqs], high) + dot_nt(q_low[seqs], high) + dot_nt(q_high[seqs], sl_v[lines])
        row = lax.broadcasted_iota(jnp.int32, (unit, 2 * HEAD_DIM), 0)
        lane = lax.broadcasted_iota(jnp.int32, (unit, 2 * HEAD_DIM), 1)
        total = jnp.zeros((unit, 2 * HEAD_DIM), F32)
        for j in range(unit // 2):
            own = row == 2 * j + lane // HEAD_DIM
            total = total + jnp.where(own, prod[:, 128 * j : 128 * j + 128], 0.0)
        pieces.append((total + swap(total))[:, :HEAD_DIM])
    state_query = jnp.concatenate(pieces, axis=0)
    read_out = decay * state_query + (step * key_query + skip) * values
    gated = read_out * silu(gate_z)
    gated = gated * lax.rsqrt(jnp.mean(gated * gated, axis=1, keepdims=True) + EPS)
    mixed = (gated * hg_v[...]).astype(BF16)
    part[:rows, :] = dot(mixed, wo_v[...])
    for i in range(nt // 2):
        a, b = pack(part[:rows, 128 * i : 128 * i + 128])
        s2[2 * i] = a.astype(BF16)
        s2[2 * i + 1] = b.astype(BF16)
    exchange(1, "tp", tp_peer, nt, lambda peer: s2.at[peer], r2, tp)
    r2[tp] = s2[tp]
    landed(1, r2, nt, recv_sem)
    summed = r2[0].astype(F32)
    for i in range(1, nt):
        summed = summed + r2[i].astype(F32)
    residual = (tok_packed + summed).astype(BF16).astype(F32)

    turned = swap(residual)
    placed = jnp.concatenate(
        [
            jnp.where(low, residual, 0.0),
            jnp.where(low, turned, 0.0),
            jnp.where(low, 0.0, turned),
            jnp.where(low, 0.0, residual),
        ],
        axis=0,
    ).astype(BF16)
    slots = dot(pt_v[...], placed)
    for q in range(EXP_IN):
        s3f[:, q, :] = slots[q * ne : (q + 1) * ne]
    s3[...] = s3f[...].astype(BF16)
    exchange(2, "ep", ep_peer, ne, lambda peer: s3.at[peer], r3, ep)
    r3[ep] = s3[ep]
    landed(2, r3, ne, recv_sem)

    r3f[...] = r3[...].astype(F32)
    for q in range(EXP_IN):
        s4[q] = r3f[:, q, :].astype(BF16)
    exchange(3, "tp", tp_peer, nt, lambda peer: s4.at[peer // share_tp], g4, tp)
    g4[tp] = s4[tp // share_tp]
    for copy in load_ffn:
        copy.wait()
    landed(3, g4, nt, recv_sem)
    blocks = []
    square = jnp.zeros((2 * ne, 2 * HEAD_DIM), F32)
    for i in range(nt // 2):
        block = unpack(g4[2 * i].astype(F32), g4[2 * i + 1].astype(F32))
        square = square + block * block
        blocks.append(block)
    scale = lax.rsqrt(jnp.sum(square, axis=1, keepdims=True) / width + EPS)
    for i, block in enumerate(blocks):
        cols = slice(128 * i, 128 * i + 128)
        part[: 2 * ne, cols] = block * scale * fg_v[:, cols]
    ffn_in = part[: 2 * ne, :].astype(BF16)
    hidden = (silu(dot(ffn_in, eg_v[...])) * dot(ffn_in, eu_v[...])).astype(BF16)
    part[: 2 * ne, :] = dot(hidden, ed_v[...])
    for i in range(nt // 2):
        a, b = pack(part[: 2 * ne, 128 * i : 128 * i + 128])
        s5[2 * i] = a.astype(BF16)
        s5[2 * i + 1] = b.astype(BF16)
    exchange(4, "tp", tp_peer, nt, lambda peer: s5.at[peer], r5, tp)
    r5[tp] = s5[tp]
    landed(4, r5, nt, recv_sem)
    for q in range(EXP_IN):
        total = r5[q * share_tp].astype(F32)
        for i in range(1, share_tp):
            total = total + r5[q * share_tp + i].astype(F32)
        s6f[:, q, :] = total
    s6[...] = s6f[...].astype(BF16)
    exchange(5, "ep", ep_peer, ne, lambda peer: s6.at[peer], r6, ep)
    r6[ep] = s6[ep]
    landed(5, r6, ne, recv_sem)
    r3f[...] = r6[...].astype(F32)
    back = jnp.concatenate([r3f[:, q, :] for q in range(EXP_IN)], axis=0)
    back = jnp.concatenate([back, swap(back)], axis=0).astype(BF16)
    each = dot(pk_v[...], back)
    moe = share_col[0] * each[:rows] + share_col[1] * each[rows:]
    plain = jnp.concatenate([residual, swap(residual)], axis=0)
    out_ref[...] = (plain + moe)[:, :HEAD_DIM].astype(BF16)

    for phase, (ref, count) in enumerate(((g1, nt), (s2, nt), (s3, ne), (g4, nt), (s5, nt), (s6, ne))):
        landed(phase, ref, count, send_sem)


def local(nx, *args):
    (
        tokens, mix_gain, w_gate, w_value, w_key, w_query, w_step, step_bias, decay_log, skip_gain,
        conv_x, conv_b, conv_c, window_x, window_b, window_c, state, head_gain, w_out, ffn_gain,
        route_ids, route_weights, e_gate, e_up, e_down,
    ) = args
    ne, nt = lax.axis_size("ep"), lax.axis_size("tp")
    rows = tokens.shape[0]
    half = rows // 2
    width = nt * HEAD_DIM
    experts = EXP_IN * ne
    operands = (
        tokens, mix_gain[None], w_gate.T, w_value.T, w_key, w_query, w_step.T,
        step_bias[None], decay_log[None], skip_gain[None],
        conv_x, conv_b, conv_c,
        window_x.transpose(1, 0, 2), window_b.transpose(1, 0, 2), window_c.transpose(1, 0, 2),
        state.reshape(rows * HEAD_DIM, STATE), head_gain[None], w_out, ffn_gain[None],
        route_ids.T, route_weights.T, e_gate[0], e_up[0], e_down[0],
    )
    tall = max(rows, 2 * ne)
    hidden = e_gate.shape[2]
    vmem = pltpu.VMEM
    scratch = [
        vmem((rows, HEAD_DIM), BF16), vmem((1, width), F32), vmem((2 * HEAD_DIM + nt, width), BF16),
        vmem((width, 2 * STATE), BF16), vmem((1, nt), F32), vmem((1, nt), F32), vmem((1, nt), F32),
        vmem((4, HEAD_DIM), BF16), vmem((4, STATE), BF16), vmem((4, STATE), BF16),
        vmem((3, rows, HEAD_DIM), BF16), vmem((3, rows, STATE), BF16), vmem((3, rows, STATE), BF16),
        vmem((rows * HEAD_DIM, STATE), F32), vmem((1, HEAD_DIM), F32), vmem((HEAD_DIM, width), BF16),
        vmem((1, width), F32), vmem((2, rows), jnp.int32), vmem((2, rows), F32),
        vmem((width, hidden), BF16), vmem((width, hidden), BF16), vmem((hidden, width), BF16),
        vmem((half, 128), BF16), vmem((nt, half, 128), BF16),
        vmem((nt, half, 128), BF16), vmem((nt, half, 128), BF16),
        vmem((ne, EXP_IN, 128), F32), vmem((ne, EXP_IN, 128), BF16), vmem((ne, EXP_IN, 128), BF16),
        vmem((ne, EXP_IN, 128), F32),
        vmem((EXP_IN, ne, 128), BF16), vmem((nt, ne, 128), BF16),
        vmem((nt, ne, 128), BF16), vmem((nt, ne, 128), BF16),
        vmem((ne, EXP_IN, 128), F32), vmem((ne, EXP_IN, 128), BF16), vmem((ne, EXP_IN, 128), BF16),
        vmem((rows, width), BF16), vmem((tall, width), F32),
        vmem((rows * HEAD_DIM, STATE), BF16), vmem((rows * HEAD_DIM, STATE), BF16),
        vmem((experts, 2 * rows), BF16), vmem((2 * rows, 2 * experts), BF16),
        pltpu.SemaphoreType.DMA((25,)), pltpu.SemaphoreType.DMA((6,)), pltpu.SemaphoreType.DMA((6,)),
    ]
    return pl.pallas_call(
        functools.partial(kernel, ne, nt, nx, rows),
        out_shape=jax.ShapeDtypeStruct((rows, HEAD_DIM), BF16),
        in_specs=[pl.BlockSpec(memory_space=pl.ANY)] * len(operands),
        out_specs=pl.BlockSpec(memory_space=pltpu.VMEM),
        scratch_shapes=scratch,
        compiler_params=pltpu.CompilerParams(
            collective_id=0, has_side_effects=True
        ),
    )(*operands)


def solution(mesh):
    in_specs = (
        P("ep", "tp"), P(), P(None, "tp"), P(None, "tp"), P(), P(), P(), P(), P(), P(),
        P(None, "tp"), P(), P(), P("ep", None, "tp"), P("ep", None, None), P("ep", None, None),
        P("ep", "tp", None, None), P("tp"), P("tp", None), P(), P("ep", None), P("ep", None),
        P("ep", None, "tp"), P("ep", None, "tp"), P("ep", "tp", None),
    )
    return jax.shard_map(
        functools.partial(local, NX), mesh=mesh, in_specs=in_specs, out_specs=P("ep", "tp"), check_vma=False
    )
```

time: 162 us -> 75.7 us (0.47); the launches traced: 160 us -> 75.5 us
  Pallas kernels: 0 us -> 74.2 us
  blocking collectives: 60.3 us -> 0 us
  waiting for transfers between devices: 43 us -> 0 us
  starting transfers between devices: 26.3 us -> 0 us
  local copies, waits for them, and re-layouts: 14.6 us -> 1.31 us
  matrix products: 7.49 us -> 0 us
  other arithmetic: 7.21 us -> 0 us
    pallas_call x0 -> x1, Pallas kernels: none -> 74.2 us  [local(): pl.pallas_call(functools.partial(kernel, ne, nt, nx, rows), out_shape=jax...]
    all_to_all x2 -> x0, blocking collectives: 60.3 us -> none  [the longest x1 47.4 us: local(): lax.all_to_all(outgoing, 'ep', split_axis=0, concat_axis=0, tiled=True)]
    all_to_all x4 -> x0, waiting for transfers between devices: 43 us -> none  [the longest x1 21.5 us: local(): lax.all_to_all(expert_out.astype(jnp.bfloat16), 'ep', split_axis=0, conca...]
    all_to_all x4 -> x0, starting transfers between devices: 26.3 us -> none  [the longest x2 14.4 us: sent_to_all(): return lax.all_to_all(copies, axis, split_axis=0, concat_axis=0, tiled=True)]
    dot_general x12 -> x0, matrix products: 7.49 us -> none  [the longest x9 4.21 us: product(): return jnp.dot(left, right, preferred_element_type=jnp.float32)]
    dynamic_slice x3 -> x0, local copies, waits for them, and re-layouts: 3.8 us -> none  [the longest x1 1.3 us: local(): skip_heads = lax.dynamic_slice_in_dim(skip_gain, first_head, head_count, 0)]
    unnamed x43 -> x1, local copies, waits for them, and re-layouts: 4.87 us -> 1.31 us
    convert_element_type x9 -> x0, other arithmetic: 2.97 us -> none  [the longest x3 2.05 us: short_conv(): conv_taps = weight.astype(jnp.float32)]
  transfers between devices with their start and end apart: 4 -> 0, of which waited for: 4 -> 0; matrix products, arithmetic and copies ran while one was open for 6% -> 0% of each run, Pallas kernels for 0% -> 0%
where the time goes in v1:
time: 75.7 us; the launch traced here: 75.5 us
  Pallas kernels  74.2 us (98%)
  local copies, waits for them, and re-layouts  1.31 us (2%)
    pallas_call x1, Pallas kernels, local(): pl.pallas_call(functools.partial(kernel, ne, nt, nx, rows), out_shape=jax...  74.2 us

profile of v1, /device:TPU:1, one launch (start us, length us, event | category | flops | bytes accessed | tf_op | source)
XLA Modules:
  0.0 75.5 jit_solution(9922333489536999208)
XLA Ops:
  0.0 74.2 %shard_map.235 = bf16[48,64]{1,0:T(8,128)(2,1)} custom-call(bf16[48,64]{1,0:T(8,128)(2,1)} %refs_0_.1, f32[1,2048]{1,0:T(1,128)} %bitcast.28, bf16[64,2048]{1,0:T(8,128)(2,1)} %bitcast.22, bf16[64,2048]{1,0:T(8,128)(2,1)} %bitcast.23, bf16[2048,256]{1,0:T(8,128)(2,1)} %refs_4_.1, bf16[2048,256]{1,0:T(8,128)(2,1)} %refs_5_.1, bf16[32,2048]{1,0:T(8,128)(2,1)} %bitcast.24, ...), custom_call_target="tpu_custom_call" | custom-call | tf_op jit(solution)/shard_map/pallas_call | solution.py:381
  74.2 1.3 %copy.27 = bf16[48,64]{1,0:T(8,128)(2,1)} copy(bf16[48,64]{1,0:T(8,128)(2,1)} %shard_map.235) | data formatting | bytes 12288

commit v2 on v1

v2 whole, which is shorter than its diff:
```python
import functools

import jax
import jax.numpy as jnp
from jax import lax
from jax.experimental import pallas as pl
from jax.experimental.pallas import tpu as pltpu
from jax.sharding import PartitionSpec as P

MESH = pl.DeviceIdType.MESH
NX = 4
HEAD_DIM = 64
STATE = 128
GROUPS = 2
EXP_IN = 4
EPS = 1e-06
F32 = jnp.float32
BF16 = jnp.bfloat16


def far_first(i, n):
    half = lax.div(i + 1, 2)
    return n // 2 + half * (1 - 2 * lax.rem(i, 2))


def silu(v):
    return v / (1.0 + jnp.exp(-v))


def dot(a, b):
    return lax.dot_general(a, b, (((1,), (0,)), ((), ())), preferred_element_type=F32)


def dot_nt(a, b):
    return lax.dot_general(a, b, (((1,), (1,)), ((), ())), preferred_element_type=F32)


def kernel(ne, nt, nx, rows, *refs):
    (
        tokens, mix_gain, w_gate, w_value, w_key, w_query, w_step, step_bias, decay_log, skip_gain,
        conv_x, conv_b, conv_c, window_x, window_b, window_c, state, head_gain, w_out, ffn_gain,
        route_ids, route_weights, e_gate, e_up, e_down,
        out_ref,
        tok_v, mg_v, wgv_v, wall_v, bias_v, dlog_v, skip_v, cx_v, cb_v, cc_v, wx_v, wb_v, wc_v,
        st_v, hg_v, wo_v, fg_v, ids_v, rw_v, egu_v, ed_v,
        s1, g1, s2, r2, s3f, s3, r3, r3f, s4, g4, s5, r5, s6f, s6, r6,
        xbuf, nbuf, sh_v, sl_v, pt_v, pk_v,
        load_sem, send_sem, row_sem, recv_sem, near_sem, far_sem, all_sem,
    ) = refs
    ep = lax.axis_index("ep")
    tp = lax.axis_index("tp")
    ny, nz = nt // nx, ne // 2
    half = rows // 2
    eh = ne // 2
    width = nt * HEAD_DIM
    span = nx * HEAD_DIM
    experts = EXP_IN * ne
    share_tp = nt // EXP_IN
    group = tp // (nt // GROUPS)
    gcol = pl.multiple_of(group * STATE, STATE)
    ty, tx = lax.div(tp, nx), lax.rem(tp, nx)
    ez, ec = lax.div(ep, 2), lax.rem(ep, 2)
    my_half = lax.div(ep, eh)
    offsets = [nx // 2 + ((i + 1) // 2) * (1 - 2 * (i % 2)) for i in range(nx)]
    xs = [lax.rem(tx + d, nx) for d in offsets]

    def for_rows(body):
        def step(i, c):
            body(lax.rem(ty + far_first(i, ny), ny), xs)
            return c

        lax.fori_loop(0, ny - 1, step, 0)
        body(ty, xs[:-1])

    def for_sets(body):
        def step(i, c):
            z = lax.rem(ez + far_first(i, nz), nz)
            body(2 * z + 1 - ec)
            body(2 * z + ec)
            return c

        lax.fori_loop(0, nz - 1, step, 0)
        body(2 * ez + 1 - ec)

    loads = []

    def load(src, dst):
        copy = pltpu.make_async_copy(src, dst, load_sem.at[len(loads)])
        copy.start()
        loads.append(copy)
        return copy

    load_tok = load(tokens, tok_v)
    barrier = pltpu.get_barrier_semaphore()

    def greet(axis, peer):
        pl.semaphore_signal(barrier, inc=1, device_id={axis: peer}, device_id_type=MESH)

    def inside(d):
        return jnp.logical_and(ez + d >= 0, ez + d < nz)

    def reach(*steps):
        return sum(inside(d).astype(jnp.int32) for d in steps)

    def tell(sem, *steps):
        for d in steps:
            @pl.when(inside(d))
            def _():
                pl.semaphore_signal(sem, inc=1, device_id={"ep": ep + 2 * d}, device_id_type=MESH)

    for d in (2, -2, 1, -1):
        @pl.when(inside(d))
        def _():
            for c in range(2):
                greet("ep", 2 * (ez + d) + c)

    greet("ep", 2 * ez + 1 - ec)

    def greet_row(y, cols):
        for x in cols:
            greet("tp", y * nx + x)

    for_rows(greet_row)

    load_ids = load(route_ids, ids_v)
    load_rw = load(route_weights, rw_v)
    load_state = load(state, st_v)
    load_win = [
        load(window_x, wx_v),
        load(window_b.at[:, :, pl.ds(gcol, STATE)], wb_v),
        load(window_c.at[:, :, pl.ds(gcol, STATE)], wc_v),
        load(conv_x, cx_v),
        load(conv_b.at[:, pl.ds(gcol, STATE)], cb_v),
        load(conv_c.at[:, pl.ds(gcol, STATE)], cc_v),
    ]
    load_mix = [
        load(mix_gain, mg_v),
        load(w_gate, wgv_v.at[pl.ds(0, HEAD_DIM)]),
        load(w_value, wgv_v.at[pl.ds(HEAD_DIM, HEAD_DIM)]),
        load(w_step, wgv_v.at[pl.ds(2 * HEAD_DIM, w_step.shape[0])]),
        load(w_key.at[:, pl.ds(gcol, STATE)], wall_v.at[:, pl.ds(0, STATE)]),
        load(w_query.at[:, pl.ds(gcol, STATE)], wall_v.at[:, pl.ds(STATE, STATE)]),
        load(step_bias, bias_v),
        load(decay_log, dlog_v),
        load(skip_gain, skip_v),
        load(head_gain, hg_v),
        load(w_out, wo_v),
    ]
    hidden_w = e_gate.shape[1]
    load_ffn = [
        load(ffn_gain, fg_v),
        load(e_gate, egu_v.at[:, pl.ds(0, hidden_w)]),
        load(e_up, egu_v.at[:, pl.ds(hidden_w, hidden_w)]),
        load(e_down, ed_v),
    ]

    low = lax.broadcasted_iota(jnp.int32, (1, 2 * HEAD_DIM), 1) < HEAD_DIM

    def swap(a):
        return pltpu.roll(a, HEAD_DIM, 1)

    def unpack(a, b):
        top = jnp.where(low, a, swap(b))
        bottom = jnp.where(low, swap(a), b)
        return jnp.concatenate([top, bottom], axis=0)

    def pack(block):
        n = block.shape[0] // 2
        top, bottom = block[:n], block[n:]
        return jnp.where(low, top, swap(bottom)), jnp.where(low, swap(top), bottom)

    def send_row(phase, y, cols, source, slot, sem):
        for x in cols:
            peer = y * nx + x
            pltpu.make_async_remote_copy(
                src_ref=source(peer),
                dst_ref=slot,
                send_sem=send_sem.at[phase],
                recv_sem=sem,
                device_id={"tp": peer},
                device_id_type=MESH,
            ).start()

    def send_set(phase, peer, source, slot, sem):
        pltpu.make_async_remote_copy(
            src_ref=source,
            dst_ref=slot,
            send_sem=send_sem.at[phase],
            recv_sem=sem,
            device_id={"ep": peer},
            device_id_type=MESH,
        ).start()

    def arrive(ref, sem):
        pltpu.make_async_copy(ref, ref, sem).wait()

    def rows_arrived(phase, target, start, use):
        arrive(target.at[pl.ds(0, nx - 1)], row_sem.at[phase, ty])
        carry = use(ty, start)

        def step(i, c):
            y = lax.rem(ty + far_first(ny - 2 - i, ny), ny)
            arrive(target.at[pl.ds(0, nx)], row_sem.at[phase, y])
            return use(y, c)

        return lax.fori_loop(0, ny - 1, step, carry)

    def spread_row(target, y, square):
        for j in range(nx // 2):
            block = unpack(target[y * nx + 2 * j].astype(F32), target[y * nx + 2 * j + 1].astype(F32))
            square = square + block * block
            col = y * span + 2 * HEAD_DIM * j
            if not isinstance(y, int):
                col = pl.multiple_of(col, 2 * HEAD_DIM)
            xbuf[: block.shape[0], pl.ds(col, 2 * HEAD_DIM)] = block
        return square

    def normalized(n, square, gain):
        scale = lax.rsqrt(jnp.sum(square, axis=1, keepdims=True) / width + EPS)
        for i in range(nt // 2):
            cols = slice(128 * i, 128 * i + 128)
            nbuf[:n, cols] = (xbuf[:n, cols] * scale * gain[:, cols]).astype(BF16)
        return nbuf[:n, :]

    load_tok.wait()
    tok = tok_v[...].astype(F32)
    tok_packed = jnp.concatenate([tok[:half], tok[half:]], axis=1)
    s1[...] = tok_packed.astype(BF16)
    g1[tp] = tok_packed.astype(BF16)
    pl.semaphore_wait(barrier, 2 * reach(2, -2, 1, -1) + nt)
    for_rows(lambda y, cols: send_row(0, y, cols, lambda peer: s1, g1.at[tp], row_sem.at[0, ty]))
    tell(near_sem, 2, -2)

    load_ids.wait()
    load_rw.wait()
    line = lax.broadcasted_iota(jnp.int32, (experts, rows), 0)
    expert_of = (line % ne) * EXP_IN + line // ne
    ids = ids_v[...]
    hit = [(ids[k : k + 1] == expert_of).astype(F32) for k in range(2)]
    named = (hit[0] + hit[1]).astype(BF16)
    before = (
        lax.broadcasted_iota(jnp.int32, (rows, rows), 0) < lax.broadcasted_iota(jnp.int32, (rows, rows), 1)
    ).astype(BF16)
    earlier = dot(named, before)
    rank = [(earlier < 0.5).astype(F32), (earlier > 0.5).astype(F32)]
    for r in range(2):
        pt_v[:, r * rows : (r + 1) * rows] = (named.astype(F32) * rank[r]).astype(BF16)
    for k in range(2):
        for r in range(2):
            pk_v[k * rows : (k + 1) * rows, r * experts : (r + 1) * experts] = (
                jnp.transpose(hit[k] * rank[r]).astype(BF16)
            )
    rw = rw_v[...]
    share = rw / jnp.sum(rw, axis=0, keepdims=True)
    eye = (
        lax.broadcasted_iota(jnp.int32, (rows, rows), 0) == lax.broadcasted_iota(jnp.int32, (rows, rows), 1)
    )
    share_col = [
        jnp.sum(jnp.where(eye, share[k : k + 1], 0.0), axis=1, keepdims=True) for k in range(2)
    ]
    load_state.wait()
    st = st_v[...]
    st_high = st.astype(BF16)
    sh_v[...] = st_high
    sl_v[...] = (st - st_high.astype(F32)).astype(BF16)
    for copy in load_win:
        copy.wait()

    def taps(window, weight):
        w = weight[...].astype(F32)
        total = window[0].astype(F32) * w[0:1]
        for j in range(1, 3):
            total = total + window[j].astype(F32) * w[j : j + 1]
        return total, w[3:4]

    past_x, tap_x = taps(wx_v, cx_v)
    past_b, tap_b = taps(wb_v, cb_v)
    past_c, tap_c = taps(wc_v, cc_v)
    for copy in load_mix:
        copy.wait()
    wall_v[:, 2 * STATE :] = jnp.transpose(wgv_v[...])
    mine = lax.broadcasted_iota(jnp.int32, (1, nt), 1) == tp

    def head_scalar(ref):
        return jnp.sum(jnp.where(mine, ref[...], 0.0), axis=1, keepdims=True)

    bias = head_scalar(bias_v)
    decay_rate = jnp.exp(head_scalar(dlog_v))
    skip = head_scalar(skip_v)

    pl.semaphore_wait(near_sem, reach(2, -2))
    tell(far_sem, 4, -4)
    def spread():
        pl.semaphore_wait(far_sem, reach(4, -4))
        pl.semaphore_signal(
            all_sem, inc=1, device_id={"ep": lax.rem(ep + eh, ne)}, device_id_type=MESH
        )

    pl.when(my_half == 1)(spread)

    square = rows_arrived(
        0, g1, jnp.zeros((rows, 2 * HEAD_DIM), F32), lambda y, c: spread_row(g1, y, c)
    )
    both = dot(normalized(rows, square, mg_v), wall_v[...])
    kq, gvs = both[:, : 2 * STATE], both[:, 2 * STATE :]
    gate_z = gvs[:, :HEAD_DIM]
    raw_v = gvs[:, HEAD_DIM : 2 * HEAD_DIM]
    keys = silu(past_b + kq[:, :STATE] * tap_b)
    queries = silu(past_c + kq[:, STATE:] * tap_c)
    values = silu(past_x + raw_v * tap_x)
    step_in = jnp.sum(jnp.where(mine, gvs[:, 2 * HEAD_DIM :], 0.0), axis=1, keepdims=True) + bias
    step = jnp.maximum(step_in, 0.0) + jnp.log1p(jnp.exp(-jnp.abs(step_in)))
    decay = jnp.exp(-step * decay_rate)
    key_query = jnp.sum(keys * queries, axis=1, keepdims=True)
    q_high = queries.astype(BF16)
    q_low = (queries - q_high.astype(F32)).astype(BF16)
    pieces = []
    unit = min(8, rows)
    for g in range(rows // unit):
        seqs = slice(g * unit, (g + 1) * unit)
        lines = slice(g * unit * HEAD_DIM, (g + 1) * unit * HEAD_DIM)
        both = jnp.concatenate([q_high[seqs].astype(F32), q_low[seqs].astype(F32)], axis=0).astype(BF16)
        prod = dot_nt(both, sh_v[lines])
        prod = prod[:unit] + prod[unit:] + dot_nt(q_high[seqs], sl_v[lines])
        row = lax.broadcasted_iota(jnp.int32, (unit, 2 * HEAD_DIM), 0)
        lane = lax.broadcasted_iota(jnp.int32, (unit, 2 * HEAD_DIM), 1)
        total = jnp.zeros((unit, 2 * HEAD_DIM), F32)
        for j in range(unit // 2):
            own = row == 2 * j + lane // HEAD_DIM
            total = total + jnp.where(own, prod[:, 128 * j : 128 * j + 128], 0.0)
        pieces.append((total + swap(total))[:, :HEAD_DIM])
    state_query = jnp.concatenate(pieces, axis=0)
    read_out = decay * state_query + (step * key_query + skip) * values
    gated = read_out * silu(gate_z)
    gated = gated * lax.rsqrt(jnp.mean(gated * gated, axis=1, keepdims=True) + EPS)
    mixed = (gated * hg_v[...]).astype(BF16)

    def packed_product(left, right, target):
        out = dot(left, right[...])
        for j in range(nt // 2):
            a, b = pack(out[:, 128 * j : 128 * j + 128])
            target[2 * j] = a.astype(BF16)
            target[2 * j + 1] = b.astype(BF16)

    packed_product(mixed, wo_v, s2)
    for_rows(lambda y, cols: send_row(1, y, cols, lambda peer: s2.at[peer], r2.at[tp], row_sem.at[1, ty]))
    r2[tp] = s2[tp]
    pl.when(my_half == 0)(spread)

    def add_row(y, total):
        for x in range(nx):
            total = total + r2[y * nx + x].astype(F32)
        return total

    summed = rows_arrived(1, r2, jnp.zeros((half, 2 * HEAD_DIM), F32), add_row)
    residual = (tok_packed + summed).astype(BF16).astype(F32)
    turned = swap(residual)
    placed = jnp.concatenate(
        [
            jnp.where(low, residual, 0.0),
            jnp.where(low, turned, 0.0),
            jnp.where(low, 0.0, turned),
            jnp.where(low, 0.0, residual),
        ],
        axis=0,
    ).astype(BF16)
    slots = dot(pt_v[...], placed)
    for q in range(EXP_IN):
        s3f[:, q, :] = slots[q * ne : (q + 1) * ne]
    s3[...] = s3f[...].astype(BF16)
    pl.semaphore_wait(all_sem, 1)
    for_sets(lambda peer: send_set(2, peer, s3.at[peer], r3.at[ep], recv_sem.at[my_half]))
    r3[ep] = s3[ep]

    def sets_arrived(h):
        @pl.when(my_half == h)
        def _():
            arrive(r3.at[pl.ds(0, eh - 1)], recv_sem.at[h])

        @pl.when(my_half != h)
        def _():
            arrive(r3.at[pl.ds(0, eh)], recv_sem.at[h])

    def gather_half(h):
        r3f[...] = r3[h * eh : (h + 1) * eh].astype(F32)
        for q in range(EXP_IN):
            s4[h, q] = r3f[:, q, :].astype(BF16)

        def row(y, cols):
            sub = lax.div(y * nx, share_tp)
            if share_tp < nx:
                send_row(3 + h, y, cols, lambda peer: s4.at[h, lax.div(peer, share_tp)], g4.at[h, tp], row_sem.at[2 + h, ty])
            else:
                send_row(3 + h, y, cols, lambda peer: s4.at[h, sub], g4.at[h, tp], row_sem.at[2 + h, ty])

        for_rows(row)
        g4[h, tp] = s4[h, lax.div(tp, share_tp)]

    def expert_half(h):
        square = rows_arrived(
            2 + h, g4.at[h], jnp.zeros((2 * eh, 2 * HEAD_DIM), F32), lambda y, c: spread_row(g4.at[h], y, c)
        )
        both = dot(normalized(2 * eh, square, fg_v), egu_v[...])
        hidden = (silu(both[:, :hidden_w]) * both[:, hidden_w:]).astype(BF16)

        packed_product(hidden, ed_v, s5.at[h])
        for_rows(
            lambda y, cols: send_row(
                5 + h, y, cols, lambda peer: s5.at[h, peer], r5.at[h, tp], recv_sem.at[2 + h]
            )
        )
        r5[h, tp] = s5[h, tp]

    def return_half(h):
        arrive(r5.at[h, pl.ds(0, nt - 1)], recv_sem.at[2 + h])
        for q in range(EXP_IN):
            total = r5[h, q * share_tp].astype(F32)
            for i in range(1, share_tp):
                total = total + r5[h, q * share_tp + i].astype(F32)
            s6f[:, q, :] = total
        s6[h * eh : (h + 1) * eh] = s6f[...].astype(BF16)

        def back(peer):
            @pl.when(lax.div(peer, eh) == h)
            def _():
                send_set(7, peer, s6.at[peer], r6.at[ep], recv_sem.at[4])

        for_sets(back)

    sets_arrived(0)
    gather_half(0)
    sets_arrived(1)
    gather_half(1)
    for copy in load_ffn:
        copy.wait()
    expert_half(0)
    expert_half(1)
    return_half(0)
    return_half(1)
    r6[ep] = s6[ep]
    arrive(r6.at[pl.ds(0, ne - 1)], recv_sem.at[4])
    s3f[...] = r6[...].astype(F32)
    back = jnp.concatenate([s3f[:, q, :] for q in range(EXP_IN)], axis=0)
    back = jnp.concatenate([back, swap(back)], axis=0).astype(BF16)
    each = dot(pk_v[...], back)
    moe = share_col[0] * each[:rows] + share_col[1] * each[rows:]
    plain = jnp.concatenate([residual, swap(residual)], axis=0)
    out_ref[...] = (plain + moe)[:, :HEAD_DIM]

    for phase, ref in enumerate(
        (
            g1.at[pl.ds(0, nt - 1)], s2.at[pl.ds(0, nt - 1)], s3.at[pl.ds(0, ne - 1)],
            g4.at[0, pl.ds(0, nt - 1)], g4.at[1, pl.ds(0, nt - 1)],
            s5.at[0, pl.ds(0, nt - 1)], s5.at[1, pl.ds(0, nt - 1)], s6.at[pl.ds(0, ne - 1)],
        )
    ):
        arrive(ref, send_sem.at[phase])


def local(nx, *args):
    (
        tokens, mix_gain, w_gate, w_value, w_key, w_query, w_step, step_bias, decay_log, skip_gain,
        conv_x, conv_b, conv_c, window_x, window_b, window_c, state, head_gain, w_out, ffn_gain,
        route_ids, route_weights, e_gate, e_up, e_down,
    ) = args
    ne, nt = lax.axis_size("ep"), lax.axis_size("tp")
    rows = tokens.shape[0]
    half = rows // 2
    width = nt * HEAD_DIM
    experts = EXP_IN * ne
    operands = (
        tokens, mix_gain[None], w_gate.T, w_value.T, w_key, w_query, w_step.T,
        step_bias[None], decay_log[None], skip_gain[None],
        conv_x, conv_b, conv_c,
        window_x.transpose(1, 0, 2), window_b.transpose(1, 0, 2), window_c.transpose(1, 0, 2),
        state.reshape(rows * HEAD_DIM, STATE), head_gain[None], w_out, ffn_gain[None],
        route_ids.T, route_weights.T, e_gate[0], e_up[0], e_down[0],
    )
    eh = ne // 2
    hidden = e_gate.shape[2]
    vmem = pltpu.VMEM
    scratch = [
        vmem((rows, HEAD_DIM), BF16), vmem((1, width), F32), vmem((2 * HEAD_DIM + nt, width), BF16),
        vmem((width, 2 * STATE + 2 * HEAD_DIM + nt), BF16), vmem((1, nt), F32), vmem((1, nt), F32), vmem((1, nt), F32),
        vmem((4, HEAD_DIM), BF16), vmem((4, STATE), BF16), vmem((4, STATE), BF16),
        vmem((3, rows, HEAD_DIM), BF16), vmem((3, rows, STATE), BF16), vmem((3, rows, STATE), BF16),
        vmem((rows * HEAD_DIM, STATE), F32), vmem((1, HEAD_DIM), F32), vmem((HEAD_DIM, width), BF16),
        vmem((1, width), F32), vmem((2, rows), jnp.int32), vmem((2, rows), F32),
        vmem((width, 2 * hidden), BF16), vmem((hidden, width), BF16),
        vmem((half, 128), BF16), vmem((nt, half, 128), BF16),
        vmem((nt, half, 128), BF16), vmem((nt, half, 128), BF16),
        vmem((ne, EXP_IN, 128), F32), vmem((ne, EXP_IN, 128), BF16), vmem((ne, EXP_IN, 128), BF16),
        vmem((eh, EXP_IN, 128), F32),
        vmem((2, EXP_IN, eh, 128), BF16), vmem((2, nt, eh, 128), BF16),
        vmem((2, nt, eh, 128), BF16), vmem((2, nt, eh, 128), BF16),
        vmem((eh, EXP_IN, 128), F32), vmem((ne, EXP_IN, 128), BF16), vmem((ne, EXP_IN, 128), BF16),
        vmem((max(rows, 2 * eh), width), F32), vmem((max(rows, 2 * eh), width), BF16),
        vmem((rows * HEAD_DIM, STATE), BF16), vmem((rows * HEAD_DIM, STATE), BF16),
        vmem((experts, 2 * rows), BF16), vmem((2 * rows, 2 * experts), BF16),
        pltpu.SemaphoreType.DMA((25,)), pltpu.SemaphoreType.DMA((8,)),
        pltpu.SemaphoreType.DMA((4, nt // nx)), pltpu.SemaphoreType.DMA((5,)),
        pltpu.SemaphoreType.REGULAR, pltpu.SemaphoreType.REGULAR, pltpu.SemaphoreType.REGULAR,
    ]
    total = pl.pallas_call(
        functools.partial(kernel, ne, nt, nx, rows),
        out_shape=jax.ShapeDtypeStruct((rows, HEAD_DIM), F32),
        in_specs=[pl.BlockSpec(memory_space=pl.ANY)] * len(operands),
        out_specs=pl.BlockSpec(memory_space=pltpu.VMEM),
        scratch_shapes=scratch,
        compiler_params=pltpu.CompilerParams(
            collective_id=0, has_side_effects=True
        ),
    )(*operands)
    return total.astype(BF16)


def solution(mesh):
    in_specs = (
        P("ep", "tp"), P(), P(None, "tp"), P(None, "tp"), P(), P(), P(), P(), P(), P(),
        P(None, "tp"), P(), P(), P("ep", None, "tp"), P("ep", None, None), P("ep", None, None),
        P("ep", "tp", None, None), P("tp"), P("tp", None), P(), P("ep", None), P("ep", None),
        P("ep", None, "tp"), P("ep", None, "tp"), P("ep", "tp", None),
    )
    return jax.shard_map(
        functools.partial(local, NX), mesh=mesh, in_specs=in_specs, out_specs=P("ep", "tp"), check_vma=False
    )
```

time: 75.7 us -> 66.1 us (0.87)
  Pallas kernels: 74.2 us -> 64.5 us
  other arithmetic: 0 us -> 1.34 us
  local copies, waits for them, and re-layouts: 1.31 us -> 0 us
    pallas_call x1, Pallas kernels: 74.2 us -> 64.5 us  [local(): pl.pallas_call(functools.partial(kernel, ne, nt, nx, rows), out_shape=jax...]
    convert_element_type x0 -> x1, other arithmetic: none -> 1.34 us  [local(): return total.astype(BF16)]
    unnamed x1 -> x0, local copies, waits for them, and re-layouts: 1.31 us -> none
where the time goes in v2:
time: 66.1 us; the launch traced here: 65.9 us
  Pallas kernels  64.5 us (98%)
  other arithmetic  1.34 us (2%)
    pallas_call x1, Pallas kernels, local(): pl.pallas_call(functools.partial(kernel, ne, nt, nx, rows), out_shape=jax...  64.5 us
    convert_element_type x1, other arithmetic, local(): return total.astype(BF16)  1.34 us

profile of v2, /device:TPU:1, one launch (start us, length us, event | category | flops | bytes accessed | tf_op | source)
XLA Modules:
  0.0 65.9 jit_solution(14772877417550254863)
XLA Ops:
  0.0 64.5 %shard_map.235 = f32[48,64]{1,0:T(8,128)} custom-call(bf16[48,64]{1,0:T(8,128)(2,1)} %refs_0_.1, f32[1,2048]{1,0:T(1,128)} %bitcast.28, bf16[64,2048]{1,0:T(8,128)(2,1)} %bitcast.22, bf16[64,2048]{1,0:T(8,128)(2,1)} %bitcast.23, bf16[2048,256]{1,0:T(8,128)(2,1)} %refs_4_.1, bf16[2048,256]{1,0:T(8,128)(2,1)} %refs_5_.1, bf16[32,2048]{1,0:T(8,128)(2,1)} %bitcast.24, ...), custom_call_target="tpu_custom_call" | custom-call | tf_op jit(solution)/shard_map/pallas_call | solution.py:504
  64.5 1.3 %convert_element_type.3 = bf16[48,64]{1,0:T(8,128)(2,1)} convert(f32[48,64]{1,0:T(8,128)} %shard_map.235) | non-fusion elementwise | flops 3072 | bytes 18432 | tf_op jit(solution)/shard_map/convert_element_type | solution.py:514

commit v3 on v2

--- a/solution.py
+++ b/solution.py
@@ -259,10 +259,13 @@
         jnp.sum(jnp.where(eye, share[k : k + 1], 0.0), axis=1, keepdims=True) for k in range(2)
     ]
     load_state.wait()
-    st = st_v[...]
-    st_high = st.astype(BF16)
-    sh_v[...] = st_high
-    sl_v[...] = (st - st_high.astype(F32)).astype(BF16)
+    wide = rows * HEAD_DIM // 6
+    for i in range(6):
+        lines = slice(i * wide, (i + 1) * wide)
+        st = jnp.transpose(st_v[lines])
+        st_high = st.astype(BF16)
+        sh_v[:, lines] = st_high
+        sl_v[:, lines] = (st - st_high.astype(F32)).astype(BF16)
     for copy in load_win:
         copy.wait()
 
@@ -320,8 +323,8 @@
         seqs = slice(g * unit, (g + 1) * unit)
         lines = slice(g * unit * HEAD_DIM, (g + 1) * unit * HEAD_DIM)
         both = jnp.concatenate([q_high[seqs].astype(F32), q_low[seqs].astype(F32)], axis=0).astype(BF16)
-        prod = dot_nt(both, sh_v[lines])
-        prod = prod[:unit] + prod[unit:] + dot_nt(q_high[seqs], sl_v[lines])
+        prod = dot(both, sh_v[:, lines])
+        prod = prod[:unit] + prod[unit:] + dot(q_high[seqs], sl_v[:, lines])
         row = lax.broadcasted_iota(jnp.int32, (unit, 2 * HEAD_DIM), 0)
         lane = lax.broadcasted_iota(jnp.int32, (unit, 2 * HEAD_DIM), 1)
         total = jnp.zeros((unit, 2 * HEAD_DIM), F32)
@@ -400,7 +403,8 @@
         square = rows_arrived(
             2 + h, g4.at[h], jnp.zeros((2 * eh, 2 * HEAD_DIM), F32), lambda y, c: spread_row(g4.at[h], y, c)
         )
-        both = dot(normalized(2 * eh, square, fg_v), egu_v[...])
+        ffn_in = normalized(2 * eh, square, fg_v)
+        both = dot(ffn_in, egu_v[...])
         hidden = (silu(both[:, :hidden_w]) * both[:, hidden_w:]).astype(BF16)
 
         packed_product(hidden, ed_v, s5.at[h])
@@ -420,12 +424,25 @@
             s6f[:, q, :] = total
         s6[h * eh : (h + 1) * eh] = s6f[...].astype(BF16)
 
+        away = my_half != h
+        zh = nz // 2
+
         def back(peer):
-            @pl.when(lax.div(peer, eh) == h)
-            def _():
-                send_set(7, peer, s6.at[peer], r6.at[ep], recv_sem.at[4])
-
-        for_sets(back)
+            send_set(7, peer, s6.at[peer], r6.at[ep], recv_sem.at[4])
+
+        def place(i):
+            return h * zh + lax.rem(ez + far_first(i, zh) + (zh // 2) * away.astype(jnp.int32), zh)
+
+        def step(i, c):
+            z = place(i)
+            back(2 * z + 1 - ec)
+            back(2 * z + ec)
+            return c
+
+        lax.fori_loop(0, zh - 1, step, 0)
+        z = place(zh - 1)
+        back(2 * z + 1 - ec)
+        pl.when(away)(lambda: back(2 * z + ec))
 
     sets_arrived(0)
     gather_half(0)
@@ -495,7 +512,7 @@
         vmem((2, nt, eh, 128), BF16), vmem((2, nt, eh, 128), BF16),
         vmem((eh, EXP_IN, 128), F32), vmem((ne, EXP_IN, 128), BF16), vmem((ne, EXP_IN, 128), BF16),
         vmem((max(rows, 2 * eh), width), F32), vmem((max(rows, 2 * eh), width), BF16),
-        vmem((rows * HEAD_DIM, STATE), BF16), vmem((rows * HEAD_DIM, STATE), BF16),
+        vmem((STATE, rows * HEAD_DIM), BF16), vmem((STATE, rows * HEAD_DIM), BF16),
         vmem((experts, 2 * rows), BF16), vmem((2 * rows, 2 * experts), BF16),
         pltpu.SemaphoreType.DMA((25,)), pltpu.SemaphoreType.DMA((8,)),
         pltpu.SemaphoreType.DMA((4, nt // nx)), pltpu.SemaphoreType.DMA((5,)),
@@ -503,7 +520,7 @@
     ]
     total = pl.pallas_call(
         functools.partial(kernel, ne, nt, nx, rows),
-        out_shape=jax.ShapeDtypeStruct((rows, HEAD_DIM), F32),
+        out_shape=pltpu.VMEM((rows, HEAD_DIM), F32),
         in_specs=[pl.BlockSpec(memory_space=pl.ANY)] * len(operands),
         out_specs=pl.BlockSpec(memory_space=pltpu.VMEM),
         scratch_shapes=scratch,

time: 66.1 us -> 64.4 us (0.974)
  Pallas kernels: 64.5 us -> 63.6 us
  other arithmetic: 1.34 us -> 0.6 us
    pallas_call x1, Pallas kernels: 64.5 us -> 63.6 us  [local(): pl.pallas_call(functools.partial(kernel, ne, nt, nx, rows), out_shape=plt...]
    convert_element_type x1, other arithmetic: 1.34 us -> 0.6 us  [local(): return total.astype(BF16)]
where the time goes in v3:
time: 64.4 us; the launch traced here: 64.2 us
  Pallas kernels  63.6 us (99%)
    pallas_call x1, Pallas kernels, local(): pl.pallas_call(functools.partial(kernel, ne, nt, nx, rows), out_shape=plt...  63.6 us

profile of v3, /device:TPU:1, one launch (start us, length us, event | category | flops | bytes accessed | tf_op | source)
XLA Modules:
  0.0 64.2 jit_solution(3420681174930908301)
XLA Ops:
  0.0 63.6 %shard_map.235 = f32[48,64]{1,0:T(8,128)S(1)} custom-call(bf16[48,64]{1,0:T(8,128)(2,1)} %refs_0_.1, f32[1,2048]{1,0:T(1,128)} %bitcast.28, bf16[64,2048]{1,0:T(8,128)(2,1)} %bitcast.22, bf16[64,2048]{1,0:T(8,128)(2,1)} %bitcast.23, bf16[2048,256]{1,0:T(8,128)(2,1)} %refs_4_.1, bf16[2048,256]{1,0:T(8,128)(2,1)} %refs_5_.1, bf16[32,2048]{1,0:T(8,128)(2,1)} %bitcast.24, ...), custom_call_target="tpu_custom_call" | custom-call | tf_op jit(solution)/shard_map/pallas_call | solution.py:521
  63.6 0.6 convert_element_type.3
